TPU v7x, 256 devices: a whole 4x4x8 slice. The times are simulated.
256 devices in a mesh: sp: 32 (over z, y), tp: 8 (over x, core).
Axes of the slice: x: 4, y: 4, z: 8, core: 2. Of those that a mesh axis runs over, the one named last changes fastest.
Arguments:
- hidden: bfloat16 [24576, 2048], P(('sp', 'tp')), may hold values from -6 to 6
- norm_gain: float32 [2, 2048], replicated, may hold values from 0.1 to 1.9
- w_value: bfloat16 [2, 2048, 2048], P(None, 'sp', 'tp'), may hold values from -0.125 to 0.125
- w_gate: bfloat16 [2, 2048, 2048], P(None, 'sp', 'tp'), may hold values from -0.125 to 0.125
- conv_weight: float32 [2, 31, 2048], P(None, None, 'tp'), may hold values from -3 to 3
- conv_bias: float32 [2, 2048], P(None, 'tp'), may hold values from -3 to 3
- chan_gain: float32 [2, 2048], P(None, 'tp'), may hold values from 0.1 to 1.9
- chan_shift: float32 [2, 2048], P(None, 'tp'), may hold values from -3 to 3
- w_out: bfloat16 [2, 2048, 2048], P(None, 'tp', 'sp'), may hold values from -0.125 to 0.125
Outputs:
- result: bfloat16 [24576, 2048], P(('sp', 'tp'))
All inputs are finite; a program needn't handle non-finite values.
Results may differ from a plain program's by a relative error of at most 0.015.
Values may be sent and summed in bfloat16 or wider, within the bound.
No kernel may reach another device: no remote copies, remote signals or barrier semaphores. Data moves between devices by JAX's collectives and lax.ppermute only.
A program may use at most 64 MiB of HBM per device.

v0:
```python
import jax
import jax.numpy as jnp
from jax import lax
from jax.sharding import Mesh
from jax.sharding import PartitionSpec as P

SP = ("sp_0", "sp_1")
SP_TP = ("sp_0", "sp_1", "tp")
EPS = 1e-06


def sent_together(arrays, axis, dim, along):
    widths = [a.shape[along] for a in arrays]
    both = jnp.concatenate(arrays, axis=along)
    whole = lax.all_gather(both, axis, axis=dim, tiled=True)
    return tuple(jnp.split(whole, [sum(widths[:k]) for k in range(1, len(widths))], axis=along))


def shifted(shard, axis, by):
    size = lax.axis_size(axis)
    pairs = [(i, i + by) for i in range(size) if 0 <= i + by < size]
    return lax.ppermute(shard, axis, pairs)


def sent_to_all(shard, axis):
    size = lax.axis_size(axis)
    return lax.all_to_all(
        jnp.broadcast_to(shard[None], (size, *shard.shape)), axis, 0, 0, tiled=True
    )


def of_everyone(shard, axis):
    everything = sent_to_all(shard, axis)
    return jnp.sum(everything, axis=0)


def together(arrays, axis):
    ravelled, at, finished = (jnp.concatenate([a.reshape(-1) for a in arrays]), 0, [])
    running = of_everyone(ravelled, axis)
    for a in arrays:
        finished.append(running[at : at + a.size].reshape(a.shape))
        at += a.size
    return tuple(finished)


def whole_of(shard, axes, dim):
    if not axes:
        return shard
    nearer = lax.all_gather(shard, axes[-1], axis=dim, tiled=True)
    return whole_of(nearer, axes[:-1], dim)


def cut_along(shard, dim, size):
    dims = shard.shape
    tiles = shard.reshape(*dims[:dim], size, dims[dim] // size, *dims[dim + 1 :])
    return jnp.moveaxis(tiles, dim, 0)


def sum_at_owner(shard, axis, dim):
    tiles = cut_along(shard, dim, lax.axis_size(axis))
    arrived = lax.all_to_all(tiles, axis, split_axis=0, concat_axis=0, tiled=True)
    return arrived.astype(jnp.float32).sum(axis=0)


def body(hidden, norm_gain, w_value, w_gate, conv_weight, conv_bias, chan_gain, chan_shift, w_out):
    group = lax.axis_size("tp")
    own_rows = hidden.shape[0]
    chans = w_value.shape[2]
    taps = conv_weight.shape[1]
    state = hidden
    for layer in range(norm_gain.shape[0]):
        xf = state.astype(jnp.float32)
        scale = lax.rsqrt(jnp.mean(xf * xf, axis=1, keepdims=True) + EPS)
        normed = (xf * scale * norm_gain[layer][None, :]).astype(jnp.bfloat16)
        tokens = lax.all_gather(normed, "tp", axis=0, tiled=True)
        empty = jnp.zeros((tokens.shape[0], chans), jnp.float32)

        def add_both(totals, pieces, start, tokens=tokens):
            return (
                jnp.dot(tokens, pieces[0], preferred_element_type=jnp.float32),
                jnp.dot(tokens, pieces[1], preferred_element_type=jnp.float32),
            )

        lin, gate = add_both(
            (empty, empty), sent_together((w_value[layer], w_gate[layer]), SP, 0, 1), jnp.int32(0)
        )
        glu = (lin * jax.nn.sigmoid(gate)).astype(jnp.bfloat16)
        before = shifted(glu[tokens.shape[0] - (taps - 1) :], SP, 1)
        window = jnp.concatenate([before, glu], axis=0).astype(jnp.float32)
        length = tokens.shape[0]
        mixed = jnp.zeros((length, chans), jnp.float32) + conv_bias[layer][None, :]
        for tap in range(taps):
            mixed = mixed + conv_weight[layer, tap][None, :] * window[tap : tap + length]
        totals = together((jnp.sum(mixed, axis=1), jnp.sum(mixed * mixed, axis=1)), "tp")
        mean = (totals[0] / (chans * group))[:, None]
        msq = (totals[1] / (chans * group))[:, None]
        var = msq - mean * mean
        act = jax.nn.silu(
            (mixed - mean) * lax.rsqrt(var + EPS) * chan_gain[layer][None, :]
            + chan_shift[layer][None, :]
        ).astype(jnp.bfloat16)

        def project(piece, start, act=act):
            return jnp.dot(act, piece, preferred_element_type=jnp.float32)

        partial_out = project(whole_of(w_out[layer], SP, 1), jnp.int32(0))

        def take_rows(start, count, partial_out=partial_out):
            return partial_out

        update = sum_at_owner(
            take_rows(jnp.int32(0), own_rows * lax.axis_size("tp")).astype(jnp.bfloat16), "tp", 0
        )
        state = (xf + update).astype(jnp.bfloat16)
    return state


def solution(mesh):
    torus = Mesh(mesh.devices.reshape(8, 4, mesh.shape["tp"]), ("sp_0", "sp_1", "tp"))
    in_specs = (
        P(SP_TP, None),
        P(),
        P(None, SP, "tp"),
        P(None, SP, "tp"),
        P(None, None, "tp"),
        P(None, "tp"),
        P(None, "tp"),
        P(None, "tp"),
        P(None, "tp", SP),
    )
    out_specs = P(SP_TP, None)
    return jax.shard_map(body, mesh=torus, in_specs=in_specs, out_specs=out_specs, check_vma=False)
```

profile of v0, /device:TPU:1, one launch (start us, length us, event | category | flops | bytes accessed | tf_op | source)
XLA Modules:
  0.0 361.9 jit_solution(7405386278213270947)
XLA Ops:
  8.1 1.2 fusion.14
  9.2 0.8 fusion.112
  10.1 1.9 fusion.16
  12.8 11.2 %all-gather = bf16[1,256,256]{1,2,0:T(8,128)(2,1)} all-gather(bf16[1,256,64]{1,2,0:T(8,128)(2,1)S(1)} %get-tuple-element.17), channel_id=2, replica_groups=mesh['sp_0'=8,'sp_1'=4,'tp'=8] {'sp_1'}, dimensions={2}, use_global_device_ids=true | all-gather | bytes 163840 | tf_op jit(solution)/shard_map/all_gather | solution.py:49
  24.7 0.9 fusion.110
  25.6 0.9 fusion.109
  28.0 59.0 %all-gather.13.cloned.1.call-done = bf16[2048,512]{1,0:T(8,128)(2,1)} async-done(((bf16[64,512]{1,0:T(8,128)(2,1)}), bf16[2048,512]{1,0:T(8,128)(2,1)}) %all-gather.13.cloned.1.call-update) | async-done | bytes 2097168 | tf_op jit(solution)/shard_map/all_gather | solution.py:15
  87.1 34.3 %all-gather.11.cloned.1.call-done = bf16[768,2048]{1,0:T(8,128)(2,1)} async-done(((bf16[96,2048]{1,0:T(8,128)(2,1)}), bf16[768,2048]{1,0:T(8,128)(2,1)}) %all-gather.11.cloned.1.call-update) | async-done | bytes 3145744 | tf_op jit(solution)/shard_map/all_gather | solution.py:75
  121.4 3.3 fusion.3
  124.7 1.0 fusion.6
  125.8 3.1 collective-permute-start
  128.9 0.8 collective-permute-done
  129.8 3.5 fusion.103
  134.0 4.4 %all-to-all-start = ((f32[8,1,1536]{2,1,0:T(1,128)}), f32[8,1,1536]{2,1,0:T(1,128)S(1)}, u32[]{:S(2)}, u32[]{:S(2)}) async-start(f32[8,1,1536]{2,1,0:T(1,128)} %broadcast_in_dim.4), calls=%async_computation | async-start | bytes 98304 | tf_op jit(solution)/shard_map/all_to_all | solution.py:27
  138.4 4.8 %all-to-all-done = f32[8,1,1536]{2,1,0:T(1,128)S(1)} async-done(((f32[8,1,1536]{2,1,0:T(1,128)}), f32[8,1,1536]{2,1,0:T(1,128)S(1)}, u32[]{:S(2)}, u32[]{:S(2)}) %all-to-all-start) | async-done | bytes 49184 | tf_op jit(solution)/shard_map/all_to_all | solution.py:27
  143.3 13.7 %all-gather.19.cloned.1.call-done = bf16[1,256,2048]{1,2,0:T(8,128)(2,1)} async-done(((bf16[1,256,256]{1,2,0:T(8,128)(2,1)}), bf16[1,256,2048]{1,2,0:T(8,128)(2,1)}) %all-gather.19.cloned.1.call-update) | async-done | bytes 1048592 | tf_op jit(solution)/shard_map/all_gather | solution.py:49
  156.9 2.3 convolution_convert_fusion.1
  159.3 46.4 %all_to_all.22 = bf16[8,96,2048]{2,1,0:T(8,128)(2,1)S(1)} all-to-all(bf16[8,96,2048]{2,1,0:T(8,128)(2,1)S(1)} %bitcast.90), channel_id=1, replica_groups=mesh['sp_0'=8,'sp_1'=4,'tp'=8] {'tp'}, dimensions={0} | all-to-all | bytes 6291456 | tf_op jit(solution)/shard_map/all_to_all | solution.py:61
  206.9 0.9 fusion.20
  207.9 11.0 %all-gather.2 = bf16[1,256,256]{1,2,0:T(8,128)(2,1)} all-gather(bf16[1,256,64]{1,2,0:T(8,128)(2,1)S(1)} %get-tuple-element.18), channel_id=4, replica_groups=mesh['sp_0'=8,'sp_1'=4,'tp'=8] {'sp_1'}, dimensions={2}, use_global_device_ids=true | all-gather | bytes 163840 | tf_op jit(solution)/shard_map/all_gather | solution.py:49
  219.0 16.4 %all-gather.17.cloned.1.call-done = bf16[2048,512]{1,0:T(8,128)(2,1)} async-done(((bf16[64,512]{1,0:T(8,128)(2,1)}), bf16[2048,512]{1,0:T(8,128)(2,1)}) %all-gather.17.cloned.1.call-update) | async-done | bytes 2097168 | tf_op jit(solution)/shard_map/all_gather | solution.py:15
  235.4 34.2 %all-gather.15.cloned.1.call-done = bf16[768,2048]{1,0:T(8,128)(2,1)} async-done(((bf16[96,2048]{1,0:T(8,128)(2,1)}), bf16[768,2048]{1,0:T(8,128)(2,1)}) %all-gather.15.cloned.1.call-update) | async-done | bytes 3145744 | tf_op jit(solution)/shard_map/all_gather | solution.py:75
  269.6 3.3 fusion.5
  272.9 1.0 fusion.7
  273.9 3.1 collective-permute-start.1
  277.0 0.9 fusion.108
  278.0 3.5 fusion.102
  281.6 8.6 %all_to_all.23 = f32[8,1,1536]{2,1,0:T(1,128)S(1)} all-to-all(f32[8,1,1536]{2,1,0:T(1,128)S(1)} %broadcast_in_dim.5), channel_id=1, replica_groups=mesh['sp_0'=8,'sp_1'=4,'tp'=8] {'tp'}, dimensions={0} | all-to-all | bytes 98304 | tf_op jit(solution)/shard_map/all_to_all | solution.py:27
  290.3 13.9 %all-gather.21.cloned.1.call-done = bf16[1,256,2048]{1,2,0:T(8,128)(2,1)} async-done(((bf16[1,256,256]{1,2,0:T(8,128)(2,1)}), bf16[1,256,2048]{1,2,0:T(8,128)(2,1)}) %all-gather.21.cloned.1.call-update) | async-done | bytes 1048592 | tf_op jit(solution)/shard_map/all_gather | solution.py:49
  304.2 2.3 convolution_convert_fusion
  306.5 47.1 %all_to_all.24 = bf16[8,96,2048]{2,1,0:T(8,128)(2,1)S(1)} all-to-all(bf16[8,96,2048]{2,1,0:T(8,128)(2,1)S(1)} %bitcast.91), channel_id=1, replica_groups=mesh['sp_0'=8,'sp_1'=4,'tp'=8] {'tp'}, dimensions={0} | all-to-all | bytes 6291456 | tf_op jit(solution)/shard_map/all_to_all | solution.py:61
  354.2 0.8 fusion.21
  (52 shorter events, 7.4 us)
Async XLA Ops:
  6.5 80.5 %all-gather.13.cloned.1.call-start = ((), (), s32[]{:S(2)}) async-start(), calls=%async_computation.5 | async-start | bytes 2162688 | tf_op jit(solution)/shard_map/all_gather | solution.py:15
  8.0 113.4 %all-gather.11.cloned.1.call-start = ((), (), s32[]{:S(2)}) async-start(), calls=%async_computation.4 | async-start | bytes 3538944 | tf_op jit(solution)/shard_map/all_gather | solution.py:75
  12.0 144.9 %all-gather.19.cloned.1.call-start = ((), (), s32[]{:S(2)}) async-start(), calls=%async_computation.8 | async-start | bytes 1179648 | tf_op jit(solution)/shard_map/all_gather | solution.py:49
  24.0 211.3 %all-gather.17.cloned.1.call-start = ((), (), s32[]{:S(2)}) async-start(), calls=%async_computation.7 | async-start | bytes 2162688 | tf_op jit(solution)/shard_map/all_gather | solution.py:15
  87.1 37.6 %copy-start.6 = (bf16[2048,512]{1,0:T(8,128)(2,1)S(1)}, bf16[2048,512]{1,0:T(8,128)(2,1)}, u32[]{:S(2)}) copy-start(bf16[2048,512]{1,0:T(8,128)(2,1)} %all-gather.13.cloned.1.call-done) | copy-start | bytes 6291460
  121.4 3.3 copy-start.3
  124.7 4.2 %copy-start.1 = (f32[2,256]{1,0:T(2,128)S(1)}, f32[2,256]{1,0:T(2,128)}, u32[]{:S(2)}) copy-start(f32[2,256]{1,0:T(2,128)} %param.15) | copy-start | bytes 6148
  125.8 4.0 %collective-permute-start = (bf16[30,256]{1,0:T(8,128)(2,1)S(1)}, bf16[30,256]{1,0:T(8,128)(2,1)S(1)}, u32[]{:S(2)}, u32[]{:S(2)}) collective-permute-start(bf16[30,256]{1,0:T(8,128)(2,1)S(1)} %slice.576), channel_id=1, source_target_pairs={{0,8},{8,16},{16,24},{24,32},{32,40},{40,48},{48,56},{56,64},{64,7... | collective-permute-start | bytes 46088 | tf_op jit(solution)/shard_map/ppermute | solution.py:22
  129.8 8.6 %copy-start.2 = (f32[2,256]{1,0:T(2,128)S(1)}, f32[2,256]{1,0:T(2,128)}, u32[]{:S(2)}) copy-start(f32[2,256]{1,0:T(2,128)} %param.16) | copy-start | bytes 6148
  134.0 9.2 %all-to-all-start = ((f32[8,1,1536]{2,1,0:T(1,128)}), f32[8,1,1536]{2,1,0:T(1,128)S(1)}, u32[]{:S(2)}, u32[]{:S(2)}) async-start(f32[8,1,1536]{2,1,0:T(1,128)} %broadcast_in_dim.4), calls=%async_computation | async-start | bytes 98304 | tf_op jit(solution)/shard_map/all_to_all | solution.py:27
  138.4 131.2 %all-gather.15.cloned.1.call-start = ((), (), s32[]{:S(2)}) async-start(), calls=%async_computation.6 | async-start | bytes 3538944 | tf_op jit(solution)/shard_map/all_gather | solution.py:75
  205.7 1.0 copy-start
  207.8 96.4 %all-gather.21.cloned.1.call-start = ((), (), s32[]{:S(2)}) async-start(), calls=%async_computation.9 | async-start | bytes 1179648 | tf_op jit(solution)/shard_map/all_gather | solution.py:49
  235.4 37.5 %copy-start.5 = (bf16[2048,512]{1,0:T(8,128)(2,1)S(1)}, bf16[2048,512]{1,0:T(8,128)(2,1)}, u32[]{:S(2)}) copy-start(bf16[2048,512]{1,0:T(8,128)(2,1)} %all-gather.17.cloned.1.call-done) | copy-start | bytes 6291460
  269.6 3.3 copy-start.4
  273.9 4.0 %collective-permute-start.1 = (bf16[30,256]{1,0:T(8,128)(2,1)S(1)}, bf16[30,256]{1,0:T(8,128)(2,1)S(1)}, u32[]{:S(2)}, u32[]{:S(2)}) collective-permute-start(bf16[30,256]{1,0:T(8,128)(2,1)S(1)} %slice.610), channel_id=1, source_target_pairs={{0,8},{8,16},{16,24},{24,32},{32,40},{40,48},{48,56},{56,64},{64,7... | collective-permute-start | bytes 46088 | tf_op jit(solution)/shard_map/ppermute | solution.py:22
Sparse Core Ops, SparseCore 0:
  9.9 77.1 all-gather.12
  88.9 32.4 all-gather.10
  123.2 33.7 all-gather.18
  159.4 75.9 all-gather.16
  237.0 32.4 all-gather.14
  271.2 32.9 all-gather.20
where the time goes:
time: 363 us; the launch traced here: 362 us
  waiting for transfers between devices  177 us (49%)
  blocking collectives  124 us (34%)
  other arithmetic  14.7 us (4%)
  between operations  13.7 us (4%)
  matrix products  13.3 us (4%)
  starting transfers between devices  10.8 us (3%)
  local copies, waits for them, and re-layouts  7.75 us (2%)
    all_to_all x2, blocking collectives, sum_at_owner(): lax.all_to_all(tiles, axis, split_axis=0, concat_axis=0, tiled=True)  93.5 us
    all_gather x2, waiting for transfers between devices, sent_together(): whole = lax.all_gather(both, axis, axis=dim, tiled=True)  75.5 us
    all_gather x2, waiting for transfers between devices, body(): tokens = lax.all_gather(normed, 'tp', axis=0, tiled=True)  68.5 us
    all_gather x2, waiting for transfers between devices, whole_of(): nearer = lax.all_gather(shard, axes[-1], axis=dim, tiled=True)  27.6 us
    all_gather x2, blocking collectives, whole_of(): nearer = lax.all_gather(shard, axes[-1], axis=dim, tiled=True)  22.2 us
    all_to_all x1, blocking collectives, sent_to_all(): lax.all_to_all(jnp.broadcast_to(shard[None], (size, *shard.shape)), axis,...  8.63 us
  transfers between devices with their start and end apart: 9, of which 8 were waited for; matrix products, arithmetic and copies ran while one was open for 8% of the time, Pallas kernels for 0%

commit v1 on v0

--- a/solution.py
+++ b/solution.py
@@ -72,7 +72,10 @@
         xf = state.astype(jnp.float32)
         scale = lax.rsqrt(jnp.mean(xf * xf, axis=1, keepdims=True) + EPS)
         normed = (xf * scale * norm_gain[layer][None, :]).astype(jnp.bfloat16)
-        tokens = lax.all_gather(normed, "tp", axis=0, tiled=True)
+        axis_len = lax.axis_size("tp")
+        v1 = tuple((axis_len if tick == 0 else 1 for tick in range(normed.ndim)))
+        fresh = jnp.tile(normed, v1)
+        tokens = lax.all_to_all(fresh, axis_name="tp", split_axis=0, concat_axis=0, tiled=True)
         empty = jnp.zeros((tokens.shape[0], chans), jnp.float32)
 
         def add_both(totals, pieces, start, tokens=tokens):

time: 363 us -> 308 us (0.85)
  blocking collectives: 124 us -> 79 us
  waiting for transfers between devices: 177 us -> 140 us
  starting transfers between devices: 10.8 us -> 36.8 us
    all_gather x2 -> x0, waiting for transfers between devices: 68.5 us -> none  [body(): tokens = lax.all_gather(normed, 'tp', axis=0, tiled=True)]
    all_to_all x0 -> x3, waiting for transfers between devices: none -> 68.5 us  [the longest x1 36 us: sum_at_owner(): lax.all_to_all(tiles, axis, split_axis=0, concat_axis=0, tiled=True)]
    all_to_all x2 -> x1, blocking collectives: 93.5 us -> 47.2 us  [sum_at_owner(): lax.all_to_all(tiles, axis, split_axis=0, concat_axis=0, tiled=True)]
    all_gather x2, waiting for transfers between devices: 75.5 us -> 46.5 us  [sent_together(): whole = lax.all_gather(both, axis, axis=dim, tiled=True)]
    all_to_all x0 -> x3, starting transfers between devices: none -> 21.4 us  [the longest x2 11.4 us: body(): lax.all_to_all(fresh, axis_name='tp', split_axis=0, concat_axis=0, tiled=...]
    all_gather x2, waiting for transfers between devices: 27.6 us -> 20.6 us  [whole_of(): nearer = lax.all_gather(shard, axes[-1], axis=dim, tiled=True)]
    all_to_all x1, starting transfers between devices: 4.37 us -> 9.89 us  [sent_to_all(): lax.all_to_all(jnp.broadcast_to(shard[None], (size, *shard.shape)), axis,...]
    another operation x0 -> x2, local copies, waits for them, and re-layouts: none -> 4.06 us  [body(): fresh = jnp.tile(normed, v1)]
  transfers between devices with their start and end apart: 9 -> 10, of which waited for: 8 -> 9; matrix products, arithmetic and copies ran while one was open for 8% -> 9% of each run, Pallas kernels for 0% -> 0%
where the time goes in v1:
time: 308 us
  waiting for transfers between devices  140 us (45%)
  blocking collectives  79 us (26%)
  starting transfers between devices  36.8 us (12%)
  other arithmetic  14.1 us (5%)
  between operations  13.6 us (4%)
  matrix products  13 us (4%)
  local copies, waits for them, and re-layouts  11 us (4%)
    all_to_all x1, blocking collectives, sum_at_owner(): lax.all_to_all(tiles, axis, split_axis=0, concat_axis=0, tiled=True)  47.2 us
    all_gather x2, waiting for transfers between devices, sent_together(): whole = lax.all_gather(both, axis, axis=dim, tiled=True)  46.5 us
    all_to_all x1, waiting for transfers between devices, sum_at_owner(): lax.all_to_all(tiles, axis, split_axis=0, concat_axis=0, tiled=True)  36 us
    all_to_all x2, waiting for transfers between devices, body(): lax.all_to_all(fresh, axis_name='tp', split_axis=0, concat_axis=0, tiled=...  32.5 us
    all_gather x2, blocking collectives, whole_of(): nearer = lax.all_gather(shard, axes[-1], axis=dim, tiled=True)  22.9 us
    all_gather x2, waiting for transfers between devices, whole_of(): nearer = lax.all_gather(shard, axes[-1], axis=dim, tiled=True)  20.6 us
    all_to_all x2, starting transfers between devices, body(): lax.all_to_all(fresh, axis_name='tp', split_axis=0, concat_axis=0, tiled=...  11.4 us
    all_to_all x1, starting transfers between devices, sum_at_owner(): lax.all_to_all(tiles, axis, split_axis=0, concat_axis=0, tiled=True)  9.95 us
  transfers between devices with their start and end apart: 10, of which 9 were waited for; matrix products, arithmetic and copies ran while one was open for 9% of the time, Pallas kernels for 0%

profile of v1, /device:TPU:1, one launch (start us, length us, event | category | flops | bytes accessed | tf_op | source)
XLA Modules:
  0.0 307.5 jit_solution(8900195166534772395)
XLA Ops:
  6.5 1.4 slice_bitcast_fusion
  8.6 1.2 fusion.14
  10.6 1.2 fusion.16
  11.8 2.0 tile.4
  13.8 6.9 %all-to-all-start = ((bf16[8,96,2048]{2,1,0:T(8,128)(2,1)}), bf16[8,96,2048]{2,1,0:T(8,128)(2,1)S(1)}, u32[]{:S(2)}, u32[]{:S(2)}) async-start(bf16[8,96,2048]{2,1,0:T(8,128)(2,1)} %tile.4), calls=%async_computation | async-start | bytes 6291456 | tf_op jit(solution)/shard_map/all_to_all | solution.py:78
  21.4 10.5 %all-gather = bf16[1,256,256]{1,2,0:T(8,128)(2,1)} all-gather(bf16[1,256,64]{1,2,0:T(8,128)(2,1)S(1)} %get-tuple-element.17), channel_id=2, replica_groups=mesh['sp_0'=8,'sp_1'=4,'tp'=8] {'sp_1'}, dimensions={2}, use_global_device_ids=true | all-gather | bytes 163840 | tf_op jit(solution)/shard_map/all_gather | solution.py:49
  33.1 25.1 %all-to-all-done = bf16[8,96,2048]{2,1,0:T(8,128)(2,1)S(1)} async-done(((bf16[8,96,2048]{2,1,0:T(8,128)(2,1)}), bf16[8,96,2048]{2,1,0:T(8,128)(2,1)S(1)}, u32[]{:S(2)}, u32[]{:S(2)}) %all-to-all-start) | async-done | bytes 3145760 | tf_op jit(solution)/shard_map/all_to_all | solution.py:78
  58.2 28.9 %all-gather.9.cloned.1.call-done = bf16[2048,512]{1,0:T(8,128)(2,1)} async-done(((bf16[64,512]{1,0:T(8,128)(2,1)}), bf16[2048,512]{1,0:T(8,128)(2,1)}) %all-gather.9.cloned.1.call-update) | async-done | bytes 2097168 | tf_op jit(solution)/shard_map/all_gather | solution.py:15
  87.1 2.4 fusion.3
  89.5 1.0 fusion.6
  90.5 2.4 collective-permute-start
  93.9 3.5 %fusion.103 = (f32[768]{0:T(1024)S(1)}, f32[768]{0:T(1024)S(1)}, f32[768,256]{1,0:T(8,128)S(1)}) fusion(f32[798,256]{1,0:T(8,128)S(1)} %maximum_convert_fusion, f32[256]{0:T(256)S(1)} %bitcast.134, f32[256]{0:T(256)S(1)} %bitcast.135, f32[256]{0:T(256)S(1)} %bitcast.136, f32[256]{0:T(256)S(1)} %bitcast.137, f32[256]{0:T(256)S(1)} %bitcast.138, ...), kind=kLoop, calls=%fused_computation.199 | loop fusion | flops 12777984 | bytes 25204736 | tf_op jit(solution)/shard_map/reduce_sum | solution.py:97
  98.0 9.9 %all-to-all-start.1 = ((f32[8,1,1536]{2,1,0:T(1,128)}), f32[8,1,1536]{2,1,0:T(1,128)S(1)}, u32[]{:S(2)}, u32[]{:S(2)}) async-start(f32[8,1,1536]{2,1,0:T(1,128)} %broadcast_in_dim.4), calls=%async_computation.1 | async-start | bytes 98304 | tf_op jit(solution)/shard_map/all_to_all | solution.py:27
  108.5 4.2 %all-to-all-done.1 = f32[8,1,1536]{2,1,0:T(1,128)S(1)} async-done(((f32[8,1,1536]{2,1,0:T(1,128)}), f32[8,1,1536]{2,1,0:T(1,128)S(1)}, u32[]{:S(2)}, u32[]{:S(2)}) %all-to-all-start.1) | async-done | bytes 49184 | tf_op jit(solution)/shard_map/all_to_all | solution.py:27
  112.8 11.4 %all-gather.13.cloned.1.call-done = bf16[1,256,2048]{1,2,0:T(8,128)(2,1)} async-done(((bf16[1,256,256]{1,2,0:T(8,128)(2,1)}), bf16[1,256,2048]{1,2,0:T(8,128)(2,1)}) %all-gather.13.cloned.1.call-update) | async-done | bytes 1048592 | tf_op jit(solution)/shard_map/all_gather | solution.py:49
  124.2 4.0 %convolution_convert_fusion.1 = bf16[768,2048]{1,0:T(8,128)(2,1)} fusion(bf16[1,256,2048]{1,2,0:T(8,128)(2,1)} %all-gather.13.cloned.1.call-done, f32[768,256]{1,0:T(8,128)S(1)} %get-tuple-element.12, f32[256]{0:T(256)S(1)} %bitcast.167, f32[256]{0:T(256)S(1)} %bitcast.166, f32[768]{0:T(1024)S(1)} %get-tuple-element.86, f32[768]{0:T(1024)S(1)} %get-tuple-element.85), kind=kOutput, calls=%fused_computation.3 | convolution fusion | flops 808648704 | bytes 4988928 | tf_op jit(solution)/shard_map/dot_general | solution.py:107
  128.1 10.0 %all-to-all-start.2 = ((bf16[8,96,2048]{2,1,0:T(8,128)(2,1)}), bf16[8,96,2048]{2,1,0:T(8,128)(2,1)S(1)}, u32[]{:S(2)}, u32[]{:S(2)}) async-start(bf16[8,96,2048]{2,1,0:T(8,128)(2,1)} %bitcast.96), calls=%async_computation.2 | async-start | bytes 6291456 | tf_op jit(solution)/shard_map/all_to_all | solution.py:61
  138.1 1.5 pad_maximum_fusion.1
  139.6 36.0 %all-to-all-done.2 = bf16[8,96,2048]{2,1,0:T(8,128)(2,1)S(1)} async-done(((bf16[8,96,2048]{2,1,0:T(8,128)(2,1)}), bf16[8,96,2048]{2,1,0:T(8,128)(2,1)S(1)}, u32[]{:S(2)}, u32[]{:S(2)}) %all-to-all-start.2) | async-done | bytes 3145760 | tf_op jit(solution)/shard_map/all_to_all | solution.py:61
  176.5 2.0 tile.5
  178.5 4.5 %all-to-all-start.3 = ((bf16[8,96,2048]{2,1,0:T(8,128)(2,1)}), bf16[8,96,2048]{2,1,0:T(8,128)(2,1)S(1)}, u32[]{:S(2)}, u32[]{:S(2)}) async-start(bf16[8,96,2048]{2,1,0:T(8,128)(2,1)} %tile.5), calls=%async_computation.3 | async-start | bytes 6291456 | tf_op jit(solution)/shard_map/all_to_all | solution.py:78
  183.0 12.4 %all-gather.2 = bf16[1,256,256]{1,2,0:T(8,128)(2,1)} all-gather(bf16[1,256,64]{1,2,0:T(8,128)(2,1)} %get-tuple-element.18), channel_id=4, replica_groups=mesh['sp_0'=8,'sp_1'=4,'tp'=8] {'sp_1'}, dimensions={2}, use_global_device_ids=true | all-gather | bytes 163840 | tf_op jit(solution)/shard_map/all_gather | solution.py:49
  195.4 17.6 %all-gather.11.cloned.1.call-done = bf16[2048,512]{1,0:T(8,128)(2,1)} async-done(((bf16[64,512]{1,0:T(8,128)(2,1)}), bf16[2048,512]{1,0:T(8,128)(2,1)}) %all-gather.11.cloned.1.call-update) | async-done | bytes 2097168 | tf_op jit(solution)/shard_map/all_gather | solution.py:15
  213.0 7.5 %all-to-all-done.3 = bf16[8,96,2048]{2,1,0:T(8,128)(2,1)S(1)} async-done(((bf16[8,96,2048]{2,1,0:T(8,128)(2,1)}), bf16[8,96,2048]{2,1,0:T(8,128)(2,1)S(1)}, u32[]{:S(2)}, u32[]{:S(2)}) %all-to-all-start.3) | async-done | bytes 3145760 | tf_op jit(solution)/shard_map/all_to_all | solution.py:78
  220.5 2.4 fusion.5
  223.0 1.0 fusion.7
  224.0 3.1 %collective-permute-start.1 = (bf16[30,256]{1,0:T(8,128)(2,1)S(1)}, bf16[30,256]{1,0:T(8,128)(2,1)S(1)}, u32[]{:S(2)}, u32[]{:S(2)}) collective-permute-start(bf16[30,256]{1,0:T(8,128)(2,1)S(1)} %slice.610), channel_id=1, source_target_pairs={{0,8},{8,16},{16,24},{24,32},{32,40},{40,48},{48,56},{56,64},{64,7... | collective-permute-start | bytes 46088 | tf_op jit(solution)/shard_map/ppermute | solution.py:22
  228.3 3.5 %fusion.102 = (f32[768]{0:T(1024)S(1)}, f32[768]{0:T(1024)S(1)}, f32[768,256]{1,0:T(8,128)S(1)}) fusion(f32[798,256]{1,0:T(8,128)S(1)} %maximum_convert_fusion.1, f32[256]{0:T(256)S(1)} %bitcast.100, f32[256]{0:T(256)S(1)} %bitcast.101, f32[256]{0:T(256)S(1)} %bitcast.144, f32[256]{0:T(256)S(1)} %bitcast.145, f32[256]{0:T(256)S(1)} %bitcast.146, ...), kind=kLoop, calls=%fused_computation.198 | loop fusion | flops 12777984 | bytes 25204736 | tf_op jit(solution)/shard_map/reduce_sum | solution.py:97
  231.9 8.9 %all_to_all.40 = f32[8,1,1536]{2,1,0:T(1,128)S(1)} all-to-all(f32[8,1,1536]{2,1,0:T(1,128)S(1)} %broadcast_in_dim.5), channel_id=1, replica_groups=mesh['sp_0'=8,'sp_1'=4,'tp'=8] {'tp'}, dimensions={0} | all-to-all | bytes 98304 | tf_op jit(solution)/shard_map/all_to_all | solution.py:27
  240.8 9.2 %all-gather.15.cloned.1.call-done = bf16[1,256,2048]{1,2,0:T(8,128)(2,1)} async-done(((bf16[1,256,256]{1,2,0:T(8,128)(2,1)}), bf16[1,256,2048]{1,2,0:T(8,128)(2,1)}) %all-gather.15.cloned.1.call-update) | async-done | bytes 1048592 | tf_op jit(solution)/shard_map/all_gather | solution.py:49
  250.1 2.3 convolution_convert_fusion
  252.4 47.2 %all_to_all.41 = bf16[8,96,2048]{2,1,0:T(8,128)(2,1)S(1)} all-to-all(bf16[8,96,2048]{2,1,0:T(8,128)(2,1)S(1)} %bitcast.97), channel_id=1, replica_groups=mesh['sp_0'=8,'sp_1'=4,'tp'=8] {'tp'}, dimensions={0} | all-to-all | bytes 6291456 | tf_op jit(solution)/shard_map/all_to_all | solution.py:61
  (81 shorter events, 9.1 us)
Async XLA Ops:
  6.5 80.6 %all-gather.9.cloned.1.call-start = ((), (), s32[]{:S(2)}) async-start(), calls=%async_computation.6 | async-start | bytes 2162688 | tf_op jit(solution)/shard_map/all_gather | solution.py:15
  13.8 6.9 %copy-start.1 = (bf16[2,256,64]{1,2,0:T(8,128)(2,1)S(1)}, bf16[2,256,64]{1,2,0:T(8,128)(2,1)}, u32[]{:S(2)}) copy-start(bf16[2,256,64]{1,2,0:T(8,128)(2,1)} %param.17) | copy-start | bytes 196612
  13.8 18.1 %copy-start.14 = (f32[2,256]{1,0:T(2,128)S(1)}, f32[2,256]{1,0:T(2,128)}, u32[]{:S(2)}) copy-start(f32[2,256]{1,0:T(2,128)} %param.14) | copy-start | bytes 6148
  13.8 18.6 %copy-start.2 = (f32[2,31,256]{2,0,1:T(2,128)S(1)}, f32[2,31,256]{2,0,1:T(2,128)}, u32[]{:S(2)}) copy-start(f32[2,31,256]{2,0,1:T(2,128)} %param.13) | copy-start | bytes 190468
  13.8 44.4 %all-to-all-start = ((bf16[8,96,2048]{2,1,0:T(8,128)(2,1)}), bf16[8,96,2048]{2,1,0:T(8,128)(2,1)S(1)}, u32[]{:S(2)}, u32[]{:S(2)}) async-start(bf16[8,96,2048]{2,1,0:T(8,128)(2,1)} %tile.4), calls=%async_computation | async-start | bytes 6291456 | tf_op jit(solution)/shard_map/all_to_all | solution.py:78
  20.7 103.4 %all-gather.13.cloned.1.call-start = ((), (), s32[]{:S(2)}) async-start(), calls=%async_computation.8 | async-start | bytes 1179648 | tf_op jit(solution)/shard_map/all_gather | solution.py:49
  87.1 2.4 copy-start.19
  89.5 3.4 %copy-start.15 = (f32[2,256]{1,0:T(2,128)S(1)}, f32[2,256]{1,0:T(2,128)}, u32[]{:S(2)}) copy-start(f32[2,256]{1,0:T(2,128)} %param.15) | copy-start | bytes 6148
  90.5 3.2 %collective-permute-start = (bf16[30,256]{1,0:T(8,128)(2,1)S(1)}, bf16[30,256]{1,0:T(8,128)(2,1)S(1)}, u32[]{:S(2)}, u32[]{:S(2)}) collective-permute-start(bf16[30,256]{1,0:T(8,128)(2,1)S(1)} %slice.576), channel_id=1, source_target_pairs={{0,8},{8,16},{16,24},{24,32},{32,40},{40,48},{48,56},{56,64},{64,7... | collective-permute-start | bytes 46088 | tf_op jit(solution)/shard_map/ppermute | solution.py:22
  93.8 14.1 %copy-start.16 = (f32[2,256]{1,0:T(2,128)S(1)}, f32[2,256]{1,0:T(2,128)}, u32[]{:S(2)}) copy-start(f32[2,256]{1,0:T(2,128)} %param.16) | copy-start | bytes 6148
  98.0 14.7 %all-to-all-start.1 = ((f32[8,1,1536]{2,1,0:T(1,128)}), f32[8,1,1536]{2,1,0:T(1,128)S(1)}, u32[]{:S(2)}, u32[]{:S(2)}) async-start(f32[8,1,1536]{2,1,0:T(1,128)} %broadcast_in_dim.4), calls=%async_computation.1 | async-start | bytes 98304 | tf_op jit(solution)/shard_map/all_to_all | solution.py:27
  128.1 47.4 %all-to-all-start.2 = ((bf16[8,96,2048]{2,1,0:T(8,128)(2,1)}), bf16[8,96,2048]{2,1,0:T(8,128)(2,1)S(1)}, u32[]{:S(2)}, u32[]{:S(2)}) async-start(bf16[8,96,2048]{2,1,0:T(8,128)(2,1)} %bitcast.96), calls=%async_computation.2 | async-start | bytes 6291456 | tf_op jit(solution)/shard_map/all_to_all | solution.py:61
  138.1 38.0 %copy-start = (bf16[96,2048]{1,0:T(8,128)(2,1)S(1)}, bf16[96,2048]{1,0:T(8,128)(2,1)}, u32[]{:S(2)}) copy-start(bf16[96,2048]{1,0:T(8,128)(2,1)} %param.9) | copy-start | bytes 1179652
  138.1 74.9 %all-gather.11.cloned.1.call-start = ((), (), s32[]{:S(2)}) async-start(), calls=%async_computation.7 | async-start | bytes 2162688 | tf_op jit(solution)/shard_map/all_gather | solution.py:15
  178.5 42.0 %all-to-all-start.3 = ((bf16[8,96,2048]{2,1,0:T(8,128)(2,1)}), bf16[8,96,2048]{2,1,0:T(8,128)(2,1)S(1)}, u32[]{:S(2)}, u32[]{:S(2)}) async-start(bf16[8,96,2048]{2,1,0:T(8,128)(2,1)} %tile.5), calls=%async_computation.3 | async-start | bytes 6291456 | tf_op jit(solution)/shard_map/all_to_all | solution.py:78
  183.0 67.0 %all-gather.15.cloned.1.call-start = ((), (), s32[]{:S(2)}) async-start(), calls=%async_computation.9 | async-start | bytes 1179648 | tf_op jit(solution)/shard_map/all_gather | solution.py:49
  220.5 2.4 copy-start.20
  222.9 5.3 %copy-start.3 = (f32[1,1,256]{2,0,1:T(1,128)S(1)}, f32[1,1,256]{2,0,1:T(1,128)}, u32[]{:S(2)}) copy-start(f32[1,1,256]{2,0,1:T(1,128)} %get-tuple-element.38) | copy-start | bytes 3076
  222.9 5.3 %copy-start.4 = (f32[1,1,256]{2,0,1:T(1,128)S(1)}, f32[1,1,256]{2,0,1:T(1,128)}, u32[]{:S(2)}) copy-start(f32[1,1,256]{2,0,1:T(1,128)} %get-tuple-element.39) | copy-start | bytes 3076
  222.9 5.3 %copy-start.5 = (f32[1,1,256]{2,0,1:T(1,128)S(1)}, f32[1,1,256]{2,0,1:T(1,128)}, u32[]{:S(2)}) copy-start(f32[1,1,256]{2,0,1:T(1,128)} %get-tuple-element.40) | copy-start | bytes 3076
  222.9 5.3 %copy-start.6 = (f32[1,1,256]{2,0,1:T(1,128)S(1)}, f32[1,1,256]{2,0,1:T(1,128)}, u32[]{:S(2)}) copy-start(f32[1,1,256]{2,0,1:T(1,128)} %get-tuple-element.41) | copy-start | bytes 3076
  222.9 5.3 %copy-start.7 = (f32[1,1,256]{2,0,1:T(1,128)S(1)}, f32[1,1,256]{2,0,1:T(1,128)}, u32[]{:S(2)}) copy-start(f32[1,1,256]{2,0,1:T(1,128)} %get-tuple-element.42) | copy-start | bytes 3076
  222.9 5.3 %copy-start.8 = (f32[1,1,256]{2,0,1:T(1,128)S(1)}, f32[1,1,256]{2,0,1:T(1,128)}, u32[]{:S(2)}) copy-start(f32[1,1,256]{2,0,1:T(1,128)} %get-tuple-element.43) | copy-start | bytes 3076
  223.0 5.3 %copy-start.9 = (f32[1,1,256]{2,0,1:T(1,128)S(1)}, f32[1,1,256]{2,0,1:T(1,128)}, u32[]{:S(2)}) copy-start(f32[1,1,256]{2,0,1:T(1,128)} %get-tuple-element.44) | copy-start | bytes 3076
  223.0 5.3 %copy-start.10 = (f32[1,1,256]{2,0,1:T(1,128)S(1)}, f32[1,1,256]{2,0,1:T(1,128)}, u32[]{:S(2)}) copy-start(f32[1,1,256]{2,0,1:T(1,128)} %get-tuple-element.45) | copy-start | bytes 3076
  223.0 5.3 %copy-start.11 = (f32[1,1,256]{2,0,1:T(1,128)S(1)}, f32[1,1,256]{2,0,1:T(1,128)}, u32[]{:S(2)}) copy-start(f32[1,1,256]{2,0,1:T(1,128)} %get-tuple-element.46) | copy-start | bytes 3076
  223.0 5.3 %copy-start.12 = (f32[1,1,256]{2,0,1:T(1,128)S(1)}, f32[1,1,256]{2,0,1:T(1,128)}, u32[]{:S(2)}) copy-start(f32[1,1,256]{2,0,1:T(1,128)} %get-tuple-element.47) | copy-start | bytes 3076
  223.0 5.3 %copy-start.13 = (f32[1,256]{1,0:T(1,128)S(1)}, f32[1,256]{1,0:T(1,128)}, u32[]{:S(2)}) copy-start(f32[1,256]{1,0:T(1,128)} %get-tuple-element.91) | copy-start | bytes 3076
  224.0 4.0 %collective-permute-start.1 = (bf16[30,256]{1,0:T(8,128)(2,1)S(1)}, bf16[30,256]{1,0:T(8,128)(2,1)S(1)}, u32[]{:S(2)}, u32[]{:S(2)}) collective-permute-start(bf16[30,256]{1,0:T(8,128)(2,1)S(1)} %slice.610), channel_id=1, source_target_pairs={{0,8},{8,16},{16,24},{24,32},{32,40},{40,48},{48,56},{56,64},{64,7... | collective-permute-start | bytes 46088 | tf_op jit(solution)/shard_map/ppermute | solution.py:22
  228.3 21.8 %copy-start.17 = (f32[1,256]{1,0:T(1,128)S(1)}, f32[1,256]{1,0:T(1,128)}, u32[]{:S(2)}) copy-start(f32[1,256]{1,0:T(1,128)} %get-tuple-element.87) | copy-start | bytes 3076
  228.3 21.8 %copy-start.18 = (f32[1,256]{1,0:T(1,128)S(1)}, f32[1,256]{1,0:T(1,128)}, u32[]{:S(2)}) copy-start(f32[1,256]{1,0:T(1,128)} %get-tuple-element.89) | copy-start | bytes 3076
Sparse Core Ops, SparseCore 0:
  9.9 77.1 all-gather.8
  88.9 35.1 all-gather.12
  141.5 71.5 all-gather.10
  214.7 35.3 all-gather.14
